TPU v7x, 512 devices: a whole 4x4x16 slice. The times are simulated.
512 devices in a mesh: sp: 128 (over z, x, core), tp: 4 (over y).
Axes of the slice: x: 4, y: 4, z: 16, core: 2. Of those that a mesh axis runs over, the one named last changes fastest.
Arguments:
- tokens: bfloat16 [32768, 2048], P(('sp', 'tp')), may hold values from -40 to 40
- w_query: bfloat16 [2048, 1024], P(None, 'tp'), may hold values from -0.125 to 0.125
- w_key: bfloat16 [2048, 256], P(None, 'tp'), may hold values from -0.125 to 0.125
- w_value: bfloat16 [2048, 256], P(None, 'tp'), may hold values from -0.125 to 0.125
- w_out: bfloat16 [1024, 2048], P('tp'), may hold values from -0.1875 to 0.1875
- cum_gate: float32 [16, 32768], P('tp', 'sp'), may hold values from -4684 to 0, as said below
Outputs:
- layer_out: bfloat16 [32768, 2048], P(('sp', 'tp'))
Inputs may be any that keep to these rules, and one draw needn't show every extreme that they name: `cum_gate`: each head's row does not rise along the positions.
All inputs are finite; a program needn't handle non-finite values.
Results may differ from a plain program's by a relative error of at most 0.012.
Values may be sent and summed in bfloat16 or wider, within the bound.
No kernel may reach another device: no remote copies, remote signals or barrier semaphores. Data moves between devices by JAX's collectives and lax.ppermute only.
A program may use at most 64 MiB of HBM per device.

v0:
```python
import functools
import math

import jax
import jax.numpy as jnp
from jax import lax
from jax.experimental import pallas as pl
from jax.experimental.pallas import tpu as pltpu
from jax.sharding import Mesh, PartitionSpec as P

HD = 64
ROWS = 256
HALF = 128
GROUP = 4
KROWS = 80
QROWS = 144
VROWS = 72
LOG2E = math.log2(math.e)
JUMP_LIMIT = 64.0
ZERO_LIMIT = -160.0
NEG_START = -1e30
NEG_MASKED = -2e30
BF = jnp.bfloat16
F32 = jnp.float32
SWAP = ((0, 1), (1, 0))
VMEM = pl.BlockSpec(memory_space=pltpu.VMEM)
SMEM = pl.BlockSpec(memory_space=pltpu.SMEM)
HBM = pl.BlockSpec(memory_space=pltpu.HBM)


def three_parts(x):
    high = x.astype(BF)
    rest = x - high.astype(F32)
    middle = rest.astype(BF)
    low = (rest - middle.astype(F32)).astype(BF)
    return high, middle, low


def packed(x):
    return jnp.concatenate([*three_parts(x), jnp.zeros(x.shape, BF)], axis=0)


def project_kernel(x_ref, wq_ref, wk_ref, wv_ref, gate_ref, q_ref, kv_ref):
    x = x_ref[...].reshape(ROWS, x_ref.shape[2])
    across = (((1,), (1,)), ((), ()))
    query = jnp.dot(x, wq_ref[...], preferred_element_type=F32)
    both = lax.dot_general(jnp.concatenate([wk_ref[...], wv_ref[...]], axis=0), x, across, preferred_element_type=F32)
    keys = both[0:64].astype(BF)
    values = both[64:128].astype(BF)
    levels = gate_ref[...] * -LOG2E
    for part in range(2):
        starts = [y * 64 + part * 32 for y in range(4)]
        turned = jnp.concatenate([query[at : at + 32] for at in starts], axis=0).T.astype(BF)
        q_ref[part, 0:256] = turned
        own = jnp.concatenate([keys[:, at : at + 32].astype(F32) for at in starts], axis=1)
        own = turned.astype(F32).reshape(GROUP, HD, HALF) * own
        level = jnp.concatenate([levels[:, at : at + 32] for at in starts], axis=1)
        q_ref[part, 256:272] = packed(jnp.sum(own, axis=1) * (LOG2E * 0.125) + level)
    gates = packed(levels)
    for i in range(8):
        kv_ref[i, 0:64] = keys
        kv_ref[i, 64:80] = gates
        kv_ref[i, KROWS : KROWS + 64] = values


def project(x, w_query, w_key, w_value, gate):
    return pl.pallas_call(
        project_kernel,
        in_specs=[VMEM] * 5,
        out_specs=[VMEM] * 2,
        out_shape=[
            jax.ShapeDtypeStruct((2, GROUP * HD + 16, HALF), BF),
            jax.ShapeDtypeStruct((8, KROWS + 64, ROWS), BF),
        ],
        cost_estimate=pl.CostEstimate(flops=2 * 256 * 2048 * 384, bytes_accessed=3 << 20, transcendentals=0),
        name="project",
    )(x, w_query, w_key, w_value, gate)


def attend_kernel(parts, sc_ref, q0_ref, q1_ref, q2_ref, q3_ref, own_ref, swapped_ref, *refs):
    q_refs = (q0_ref, q1_ref, q2_ref, q3_ref)
    tiles = len(parts) * GROUP
    first = len(parts) == 2
    if first:
        *outs, acc, top, qa, ks, vs, jump, work, sems = refs
    else:
        acc_in, top_in, out_ref, acc, top, qa, ks, vs, jump, work, sems = refs

    def open_state():
        if first:
            acc[...] = jnp.zeros_like(acc)
            for slot, part in enumerate(parts):
                for xq in range(4):
                    rows = q_refs[xq][part, 256:272, :].astype(F32)
                    sums = rows[0:4] + rows[4:8] + rows[8:12]
                    for h in range(GROUP):
                        top[slot * GROUP + h, :, xq * HALF : (xq + 1) * HALF] = sums[h : h + 1]
        else:
            fetch = pltpu.make_async_copy(acc_in, acc.at[0:GROUP], sems.at[0])
            fetch.start()
            top[0:GROUP] = top_in[...]
            acc[GROUP] = jnp.zeros(acc.shape[1:], F32)
            fetch.wait()
        top[tiles] = jnp.zeros(top.shape[1:], F32)
        jump[...] = jnp.zeros_like(jump)

    open_state()
    row = lax.broadcasted_iota(jnp.int32, (16, 512), 0)
    query_sizes = []
    for slot, part in enumerate(parts):
        for h in range(GROUP):
            tile = slot * GROUP + h
            sizes = []
            for xq in range(4):
                cols = slice(xq * HALF, (xq + 1) * HALF)
                scaled = q_refs[xq][part, h * HD : (h + 1) * HD, :].astype(F32) * (LOG2E * 0.125)
                high = scaled.astype(BF)
                qa[tile, 0:64, cols] = high
                qa[tile, 64:128, cols] = (scaled - high.astype(F32)).astype(BF)
                sizes.append(jnp.sum(scaled * scaled, axis=0, keepdims=True))
            qa[tile, 128:144, :] = jnp.where((row < 12) & (row % 4 == h), 1.0, 0.0).astype(BF)
            query_sizes.append(jnp.max(jnp.concatenate(sizes, axis=1), axis=1, keepdims=True))
    qa[tiles] = jnp.zeros(qa.shape[1:], BF)
    key_sizes = []
    levels = []
    for b in range(8):
        sizes = []
        gates = []
        for side, ref in enumerate((own_ref, swapped_ref)):
            keys = ref[b, 0:KROWS, :].astype(F32)
            at = slice((2 * b + side) * ROWS, (2 * b + side + 1) * ROWS)
            ks[at, 0:QROWS] = jnp.concatenate([keys[0:64], keys], axis=0).T.astype(BF)
            cols = slice(side * ROWS, (side + 1) * ROWS)
            vs[b, 0:64, cols] = ref[b, KROWS : KROWS + 64, :]
            vs[b, 64:72, cols] = jnp.ones((8, ROWS), BF)
            sizes.append(jnp.sum(keys[0:64] * keys[0:64], axis=0, keepdims=True))
            gates.append(keys[64:68] + keys[68:72] + keys[72:76])
        key_sizes.append(jnp.maximum(sizes[0], sizes[1]))
        levels.append(jnp.maximum(gates[0], gates[1]))
    key_size = jnp.max(jnp.concatenate(key_sizes, axis=0), axis=1, keepdims=True)
    number = lax.broadcasted_iota(jnp.int32, (8, 1), 0)
    starts = []
    for tile in range(tiles):
        h = tile % GROUP
        level = jnp.max(jnp.concatenate([x[h : h + 1] for x in levels], axis=0), axis=1, keepdims=True)
        lowest = jnp.min(top[tile], axis=1, keepdims=True)
        bound = jnp.sqrt(key_size * query_sizes[tile]) * 1.01 + level - lowest
        starts.append(jnp.min(jnp.where(bound < ZERO_LIMIT, 8, number)))

    full = sc_ref[0]

    def enlist(plane, count):
        for tile in range(tiles):
            work[count] = plane * 16 + tile
            count = count + jnp.where(plane >= starts[tile], 1, 0)
        return count

    count = lax.fori_loop(0, full, enlist, 0)
    for j in range(3):
        work[count + j] = tiles

    def scored(plane, tile, start):
        keys = ks[pl.ds(pl.multiple_of(plane * 512, 512), 512), 0:QROWS]
        scores = jnp.dot(keys, qa[tile], preferred_element_type=F32)
        if start is None:
            return scores
        key = lax.broadcasted_iota(jnp.int32, scores.shape, 0)
        key_pos = key + jnp.where(key < ROWS, start + sc_ref[3], start - sc_ref[3])
        lane = lax.broadcasted_iota(jnp.int32, (1, 512), 1)
        base = jnp.where(
            lane < 256, jnp.where(lane < 128, sc_ref[4], sc_ref[5]), jnp.where(lane < 384, sc_ref[6], sc_ref[7])
        )
        inner = lane % HALF
        query_pos = base * 512 + sc_ref[3] + (parts[0] + tile // GROUP) * 32 + (inner // 32) * 64 + inner % 32
        return jnp.where(key_pos <= query_pos, scores, NEG_MASKED)

    def quick_step(pairs, start):
        def soften(i):
            plane, tile = pairs[i]
            scores = scored(plane, tile, start)
            old = top[tile]
            weights = jnp.exp2(scores - old).astype(BF)
            largest = jnp.max(scores, axis=0, keepdims=True)
            new = jnp.maximum(old, largest)
            top[tile] = new
            jump[...] = jnp.maximum(jump[...], largest - old)
            return weights, jnp.exp2(old - new)

        def gather(i, weights, decay):
            plane, tile = pairs[i]
            update = jnp.dot(vs[plane], weights, preferred_element_type=F32)
            acc[tile] = (acc[tile] + update) * decay

        pending = soften(0)
        for i in range(4):
            following = soften(i + 1) if i < 3 else None
            gather(i, *pending)
            pending = following

    def edge_unit(i, c):
        quick_step([(full, i * 4 + j) for j in range(4)], sc_ref[2])
        return c

    def work_unit(i, c):
        codes = [work[i * 4 + j] for j in range(4)]
        quick_step([(code // 16, code % 16) for code in codes], None)
        return c

    lax.fori_loop(0, sc_ref[1] * len(parts), edge_unit, 0)
    lax.fori_loop(0, (count + 3) // 4, work_unit, 0)

    @pl.when(jnp.max(jump[...]) > JUMP_LIMIT)
    def _():
        open_state()

        def careful(plane, start):
            def one_tile(tile, c):
                scores = scored(plane, tile, start)
                old = top[tile]
                new = jnp.maximum(old, jnp.max(scores, axis=0, keepdims=True))
                top[tile] = new
                update = jnp.dot(vs[plane], jnp.exp2(scores - new).astype(BF), preferred_element_type=F32)
                acc[tile] = acc[tile] * jnp.exp2(old - new) + update
                return c

            lax.fori_loop(0, tiles, one_tile, 0)

        def careful_whole(plane, c):
            careful(plane, None)
            return c

        def careful_edge(plane, c):
            careful(plane, sc_ref[2])
            return c

        lax.fori_loop(0, full, careful_whole, 0)
        lax.fori_loop(full, full + sc_ref[1], careful_edge, 0)

    if first:
        stores = [
            pltpu.make_async_copy(acc.at[part * GROUP : (part + 1) * GROUP], outs[2 * part], sems.at[part]) for part in parts
        ]
        for part in parts:
            stores[part].start()
            outs[2 * part + 1][...] = top[part * GROUP : (part + 1) * GROUP]
        for part in parts:
            stores[part].wait()
    else:
        for h in range(GROUP):
            total = acc[h, 64:65, :]
            some = total > 0.0
            safe = jnp.where(some, total, 1.0)
            rows = (acc[h, 0:64, :] / safe).astype(BF)
            high, middle, low = three_parts(jnp.where(some, top[h] + jnp.log2(safe), NEG_START))
            tail = jnp.concatenate([high, middle, low, jnp.zeros((5, 512), BF)], axis=0)
            for xq in range(4):
                cols = slice(xq * HALF, (xq + 1) * HALF)
                out_ref[sc_ref[4 + xq], 0:64, h * HALF : (h + 1) * HALF] = rows[:, cols]
                out_ref[sc_ref[4 + xq], 64:72, h * HALF : (h + 1) * HALF] = tail[:, cols]


def attend(scalars, queries, own, swapped, parts, state):
    tiles = len(parts) * GROUP
    acc_shape = (GROUP, VROWS, 512)
    top_shape = (GROUP, 1, 512)
    if len(parts) == 2:
        out_shape = [jax.ShapeDtypeStruct(acc_shape, F32), jax.ShapeDtypeStruct(top_shape, F32)] * 2
    else:
        out_shape = [jax.ShapeDtypeStruct((4, VROWS, 512), BF)]
    args = [scalars, *queries, own, swapped, *state]
    return pl.pallas_call(
        functools.partial(attend_kernel, parts),
        in_specs=[SMEM] + [VMEM] * 6 + [HBM, VMEM][: len(state)],
        out_specs=[HBM, VMEM] * 2 if len(parts) == 2 else [VMEM],
        out_shape=out_shape,
        scratch_shapes=[
            pltpu.VMEM((tiles + 1, *acc_shape[1:]), F32),
            pltpu.VMEM((tiles + 1, *top_shape[1:]), F32),
            pltpu.VMEM((tiles + 1, QROWS, 512), BF),
            pltpu.VMEM((16 * ROWS, 256), BF),
            pltpu.VMEM((8, VROWS, 512), BF),
            pltpu.VMEM((1, 512), F32),
            pltpu.SMEM((80,), jnp.int32),
            pltpu.SemaphoreType.DMA((2,)),
        ],
        cost_estimate=pl.CostEstimate(flops=5_000_000_000 * len(parts), bytes_accessed=4 << 20, transcendentals=8 << 20),
        compiler_params=pltpu.CompilerParams(vmem_limit_bytes=24 << 20),
        name="attend",
    )(*args)


def merged(x_ref):
    levels = []
    for s in range(4):
        high, middle, low = (x_ref[s, 64 + j : 65 + j, :].astype(F32) for j in range(3))
        levels.append(high + middle + low)
    top = jnp.maximum(jnp.maximum(levels[0], levels[1]), jnp.maximum(levels[2], levels[3]))
    shares = [jnp.exp2(level - top) for level in levels]
    total = shares[0] + shares[1] + shares[2] + shares[3]
    mixed = x_ref[0, 0:64, :].astype(F32) * shares[0]
    for s in range(1, 4):
        mixed += x_ref[s, 0:64, :].astype(F32) * shares[s]
    return mixed / total


def finish_kernel(early_ref, late_ref, w_ref, o_ref):
    for part, ref in enumerate((early_ref, late_ref)):
        mixed = merged(ref)
        half = jnp.concatenate([mixed[:, h * HALF : (h + 1) * HALF] for h in range(GROUP)], axis=0)
        out = jnp.dot(half.T.astype(BF), w_ref[...], preferred_element_type=F32).astype(BF)
        for y in range(4):
            o_ref[y, part * 32 : part * 32 + 32, :] = out[y * 32 : y * 32 + 32]


def finish(early, late, w_out):
    return pl.pallas_call(
        finish_kernel,
        in_specs=[VMEM] * 3,
        out_specs=VMEM,
        out_shape=jax.ShapeDtypeStruct((4, 64, w_out.shape[1]), BF),
        cost_estimate=pl.CostEstimate(flops=300_000_000, bytes_accessed=3 << 20, transcendentals=0),
        name="finish",
    )(early, late, w_out)


def sent_to_all(x, axis):
    copies = jnp.broadcast_to(x, (lax.axis_size(axis), *x.shape))
    return lax.all_to_all(copies, axis, split_axis=0, concat_axis=0, tiled=True)


def per_device(tokens, w_query, w_key, w_value, w_out, cum_gate):
    zh, zl, x, c = (lax.axis_index(a) for a in ("zh", "zl", "x", "c"))
    plane = zh * 2 + zl
    rows = sent_to_all(tokens, "y")
    queries, copies = project(rows, w_query, w_key.T, w_value.T, cum_gate)
    same_own = lax.all_to_all(copies, "zh", 0, 0, tiled=True)
    two, one, three = (lax.ppermute(queries, "x", [(i, (i + j) % 4) for i in range(4)]) for j in (2, 1, 3))
    same_own, gathered = lax.optimization_barrier((same_own, [queries, one, two, three]))
    other_own = lax.ppermute(same_own, "zl", SWAP)
    same_swapped = lax.ppermute(same_own, "c", SWAP)
    scalars = []
    for parity in (zl, 1 - zl):
        full = (plane - parity + 1) // 2
        numbers = [full, 1 - (plane - parity) % 2, x * 512, c * ROWS, *((x - j) % 4 for j in range(4))]
        scalars.append(jnp.stack(numbers).astype(jnp.int32))
    acc0, top0, acc1, top1 = attend(scalars[0], gathered, same_own, same_swapped, (0, 1), ())
    top0, top1, other_own = lax.optimization_barrier((top0, top1, other_own))
    other_swapped = lax.ppermute(other_own, "c", SWAP)
    (late,) = attend(scalars[1], gathered, other_own, other_swapped, (1,), (acc1, top1))
    late_shared = lax.all_to_all(late, "x", 0, 0, tiled=True)
    (early,) = attend(scalars[1], gathered, other_own, other_swapped, (0,), (acc0, top0))
    early_shared = lax.all_to_all(early, "x", 0, 0, tiled=True)
    pieces = lax.all_to_all(finish(early_shared, late_shared, w_out), "y", 0, 0, tiled=True)
    return jnp.sum(pieces.astype(F32), axis=0).astype(BF)


def solution(mesh):
    fine = Mesh(mesh.devices.reshape(8, 2, 4, 2, 4), ("zh", "zl", "x", "c", "y"))
    sp = ("zh", "zl", "x", "c")
    placed = (
        P((*sp, "y"), None),
        P(None, "y"),
        P(None, "y"),
        P(None, "y"),
        P("y", None),
        P("y", sp),
    )
    return jax.shard_map(per_device, mesh=fine, in_specs=placed, out_specs=P((*sp, "y"), None), check_vma=False)
```

profile of v0, /device:TPU:480, one launch (start us, length us, event | category | flops | bytes accessed | tf_op | source)
XLA Modules:
  0.0 228.8 jit_solution(4198895073896857119)
XLA Ops:
  0.0 1.1 broadcast_in_dim.3
  1.1 19.5 %all_to_all.25.x_ref = bf16[4,64,2048]{2,1,0:T(8,128)(2,1)} all-to-all(bf16[4,64,2048]{2,1,0:T(8,128)(2,1)S(1)} %broadcast_in_dim.3), channel_id=1, replica_groups=mesh['zh'=8,'zl'=2,'x'=4,'c'=2,'y'=4] {'y'}, dimensions={0} | all-to-all | bytes 2097152 | tf_op jit(solution)/shard_map/all_to_all | solution.py:328
  20.5 3.3 %project.1 = (bf16[2,272,128]{2,1,0:T(8,128)(2,1)}, bf16[8,144,256]{2,1,0:T(8,128)(2,1)}) custom-call(bf16[4,64,2048]{2,1,0:T(8,128)(2,1)} %all_to_all.25.x_ref, bf16[2048,256]{1,0:T(8,128)(2,1)} %wq_ref.1, bf16[64,2048]{1,0:T(8,128)(2,1)} %bitcast.12, bf16[64,2048]{1,0:T(8,128)(2,1)} %bitcast.13, f32[4,256]{1,0:T(4,128)} %gate_ref.1), custom_call_target="tpu_custom_call" | custom-call | flops 402653184 | bytes 3145728 | tf_op jit(solution)/shard_map/project/pallas_call | solution.py:67
  23.8 0.0 copy-start
  23.8 9.4 %all-to-all-start.1 = ((bf16[8,144,256]{2,1,0:T(8,128)(2,1)}), bf16[8,144,256]{2,1,0:T(8,128)(2,1)S(1)}, u32[]{:S(2)}, u32[]{:S(2)}) async-start(bf16[8,144,256]{2,1,0:T(8,128)(2,1)} %get-tuple-element.19), calls=%async_computation.1 | async-start | bytes 1179648 | tf_op jit(solution)/shard_map/all_to_all | solution.py:336
  33.2 0.0 copy-done
  33.2 3.4 %collective-permute-start = (bf16[2,272,128]{2,1,0:T(8,128)(2,1)S(1)}, bf16[2,272,128]{2,1,0:T(8,128)(2,1)S(1)}, u32[]{:S(2)}, u32[]{:S(2)}) collective-permute-start(bf16[2,272,128]{2,1,0:T(8,128)(2,1)S(1)} %copy-done), channel_id=1, source_target_pairs={{0,8},{8,16},{16,24},{24,0},{1,9},{9,17},{17,25},{25,1},{2,10},{10... | collective-permute-start | bytes 417800 | tf_op jit(solution)/shard_map/ppermute | solution.py:337
  36.6 4.6 %collective-permute-start.1 = (bf16[2,272,128]{2,1,0:T(8,128)(2,1)S(1)}, bf16[2,272,128]{2,1,0:T(8,128)(2,1)S(1)}, u32[]{:S(2)}, u32[]{:S(2)}) collective-permute-start(bf16[2,272,128]{2,1,0:T(8,128)(2,1)S(1)} %copy-done), channel_id=1, source_target_pairs={{0,16},{8,24},{16,0},{24,8},{1,17},{9,25},{17,1},{25,9},{2,18},{10... | collective-permute-start | bytes 417800 | tf_op jit(solution)/shard_map/ppermute | solution.py:337
  41.3 3.3 %collective-permute-start.2 = (bf16[2,272,128]{2,1,0:T(8,128)(2,1)S(1)}, bf16[2,272,128]{2,1,0:T(8,128)(2,1)S(1)}, u32[]{:S(2)}, u32[]{:S(2)}) collective-permute-start(bf16[2,272,128]{2,1,0:T(8,128)(2,1)S(1)} %copy-done), channel_id=1, source_target_pairs={{0,24},{8,0},{16,8},{24,16},{1,25},{9,1},{17,9},{25,17},{2,26},{10... | collective-permute-start | bytes 417800 | tf_op jit(solution)/shard_map/ppermute | solution.py:337
  44.6 0.0 collective-permute-done.q1_ref
  44.6 0.4 collective-permute-done.1.q2_ref
  45.1 3.1 %collective-permute-done.2.q3_ref = bf16[2,272,128]{2,1,0:T(8,128)(2,1)S(1)} collective-permute-done((bf16[2,272,128]{2,1,0:T(8,128)(2,1)S(1)}, bf16[2,272,128]{2,1,0:T(8,128)(2,1)S(1)}, u32[]{:S(2)}, u32[]{:S(2)}) %collective-permute-start.2) | collective-permute-done | bytes 139296 | tf_op jit(solution)/shard_map/ppermute | solution.py:337
  48.2 13.3 %all-to-all-done.1.own_ref = bf16[8,144,256]{2,1,0:T(8,128)(2,1)S(1)} async-done(((bf16[8,144,256]{2,1,0:T(8,128)(2,1)}), bf16[8,144,256]{2,1,0:T(8,128)(2,1)S(1)}, u32[]{:S(2)}, u32[]{:S(2)}) %all-to-all-start.1) | async-done | bytes 589856 | tf_op jit(solution)/shard_map/all_to_all | solution.py:336
  61.5 1.9 collective-permute-start.3
  63.5 0.1 stack.53.sc_ref
  63.6 5.7 %collective-permute-start.4 = (bf16[8,144,256]{2,1,0:T(8,128)(2,1)S(1)}, bf16[8,144,256]{2,1,0:T(8,128)(2,1)S(1)}, u32[]{:S(2)}, u32[]{:S(2)}) collective-permute-start(bf16[8,144,256]{2,1,0:T(8,128)(2,1)S(1)} %all-to-all-done.1.own_ref), channel_id=1, source_target_pairs={{0,32},{32,0},{1,33},{33,1},{2,34},{34,2},{3,35},{35,3},{4,36},{36... | collective-permute-start | bytes 1769480 | tf_op jit(solution)/shard_map/ppermute | solution.py:339
  69.3 0.0 collective-permute-done.3.swapped_ref
  69.4 19.7 %attend.3 = (f32[4,72,512]{2,1,0:T(8,128)S(1)}, f32[4,1,512]{2,1,0:T(1,128)S(1)}, f32[4,72,512]{2,1,0:T(8,128)S(1)}, f32[4,1,512]{2,1,0:T(1,128)S(1)}) custom-call(s32[8]{0:T(128)S(1)} %stack.53.sc_ref, bf16[2,272,128]{2,1,0:T(8,128)(2,1)S(1)} %copy-done, bf16[2,272,128]{2,1,0:T(8,128)(2,1)S(1)} %collective-permute-done.q1_ref, ...), custom_call_target="tpu_custom_call" | custom-call | flops 10000000000 | bytes 4194304 | tf_op jit(solution)/shard_map/attend/pallas_call | solution.py:271
  89.0 0.0 collective-permute-done.4.own_ref
  89.0 41.3 %collective-permute-start.5 = (bf16[8,144,256]{2,1,0:T(8,128)(2,1)S(1)}, bf16[8,144,256]{2,1,0:T(8,128)(2,1)S(1)}, u32[]{:S(2)}, u32[]{:S(2)}) collective-permute-start(bf16[8,144,256]{2,1,0:T(8,128)(2,1)S(1)} %collective-permute-done.4.own_ref), channel_id=1, source_target_pairs={{0,4},{4,0},{1,5},{5,1},{2,6},{6,2},{3,7},{7,3},{8,12},{12,8},{9,1... | collective-permute-start | bytes 1769480 | tf_op jit(solution)/shard_map/ppermute | solution.py:348
  130.4 0.1 stack.50.sc_ref
  130.5 1.5 collective-permute-done.5.swapped_ref
  132.0 11.2 %attend.5 = bf16[4,72,512]{2,1,0:T(8,128)(2,1)} custom-call(s32[8]{0:T(128)S(1)} %stack.50.sc_ref, bf16[2,272,128]{2,1,0:T(8,128)(2,1)S(1)} %copy-done, bf16[2,272,128]{2,1,0:T(8,128)(2,1)S(1)} %collective-permute-done.q1_ref, bf16[2,272,128]{2,1,0:T(8,128)(2,1)S(1)} %collective-permute-done.1.q2_ref, ...), custom_call_target="tpu_custom_call" | custom-call | flops 5000000000 | bytes 4194304 | tf_op jit(solution)/shard_map/attend/pallas_call | solution.py:271
  143.2 4.5 %all-to-all-start.3 = ((bf16[4,72,512]{2,1,0:T(8,128)(2,1)}), bf16[4,72,512]{2,1,0:T(8,128)(2,1)S(1)}, u32[]{:S(2)}, u32[]{:S(2)}) async-start(bf16[4,72,512]{2,1,0:T(8,128)(2,1)} %attend.5), calls=%async_computation.3 | async-start | bytes 589824 | tf_op jit(solution)/shard_map/all_to_all | solution.py:350
  147.7 10.7 %attend.4 = bf16[4,72,512]{2,1,0:T(8,128)(2,1)S(1)} custom-call(s32[8]{0:T(128)S(1)} %stack.50.sc_ref, bf16[2,272,128]{2,1,0:T(8,128)(2,1)S(1)} %copy-done, bf16[2,272,128]{2,1,0:T(8,128)(2,1)S(1)} %collective-permute-done.q1_ref, bf16[2,272,128]{2,1,0:T(8,128)(2,1)S(1)} %collective-permute-done.1.q2_ref, ...), custom_call_target="tpu_custom_call" | custom-call | flops 5000000000 | bytes 4194304 | tf_op jit(solution)/shard_map/attend/pallas_call | solution.py:271
  158.4 0.0 all-to-all-done.3.late_ref
  158.4 0.0 copy-start.1
  158.5 11.6 %all_to_all.26.early_ref = bf16[4,72,512]{2,1,0:T(8,128)(2,1)} all-to-all(bf16[4,72,512]{2,1,0:T(8,128)(2,1)S(1)} %attend.4), channel_id=1, replica_groups=mesh['zh'=8,'zl'=2,'x'=4,'c'=2,'y'=4] {'x'}, dimensions={0} | all-to-all | bytes 589824 | tf_op jit(solution)/shard_map/all_to_all | solution.py:352
  170.0 0.0 copy-done.1
  170.0 3.0 %finish.1 = bf16[4,64,2048]{2,1,0:T(8,128)(2,1)} custom-call(bf16[4,72,512]{2,1,0:T(8,128)(2,1)} %all_to_all.26.early_ref, bf16[4,72,512]{2,1,0:T(8,128)(2,1)} %copy-done.1, bf16[256,2048]{1,0:T(8,128)(2,1)} %w_ref.1), custom_call_target="tpu_custom_call" | custom-call | flops 300000000 | bytes 3145728 | tf_op jit(solution)/shard_map/finish/pallas_call | solution.py:316
  173.0 54.9 %all_to_all.27 = bf16[4,64,2048]{2,1,0:T(8,128)(2,1)S(1)} all-to-all(bf16[4,64,2048]{2,1,0:T(8,128)(2,1)} %finish.1), channel_id=1, replica_groups=mesh['zh'=8,'zl'=2,'x'=4,'c'=2,'y'=4] {'y'}, dimensions={0} | all-to-all | bytes 2097152 | tf_op jit(solution)/shard_map/all_to_all | solution.py:353
  227.9 0.9 reduce_sum.12
Async XLA Ops:
  23.8 9.4 %copy-start = (bf16[2,272,128]{2,1,0:T(8,128)(2,1)S(1)}, bf16[2,272,128]{2,1,0:T(8,128)(2,1)}, u32[]{:S(2)}) copy-start(bf16[2,272,128]{2,1,0:T(8,128)(2,1)} %get-tuple-element.21.q0_ref) | copy-start | bytes 417796
  23.8 37.7 %all-to-all-start.1 = ((bf16[8,144,256]{2,1,0:T(8,128)(2,1)}), bf16[8,144,256]{2,1,0:T(8,128)(2,1)S(1)}, u32[]{:S(2)}, u32[]{:S(2)}) async-start(bf16[8,144,256]{2,1,0:T(8,128)(2,1)} %get-tuple-element.19), calls=%async_computation.1 | async-start | bytes 1179648 | tf_op jit(solution)/shard_map/all_to_all | solution.py:336
  33.2 11.4 %collective-permute-start = (bf16[2,272,128]{2,1,0:T(8,128)(2,1)S(1)}, bf16[2,272,128]{2,1,0:T(8,128)(2,1)S(1)}, u32[]{:S(2)}, u32[]{:S(2)}) collective-permute-start(bf16[2,272,128]{2,1,0:T(8,128)(2,1)S(1)} %copy-done), channel_id=1, source_target_pairs={{0,8},{8,16},{16,24},{24,0},{1,9},{9,17},{17,25},{25,1},{2,10},{10... | collective-permute-start | bytes 417800 | tf_op jit(solution)/shard_map/ppermute | solution.py:337
  36.6 8.5 %collective-permute-start.1 = (bf16[2,272,128]{2,1,0:T(8,128)(2,1)S(1)}, bf16[2,272,128]{2,1,0:T(8,128)(2,1)S(1)}, u32[]{:S(2)}, u32[]{:S(2)}) collective-permute-start(bf16[2,272,128]{2,1,0:T(8,128)(2,1)S(1)} %copy-done), channel_id=1, source_target_pairs={{0,16},{8,24},{16,0},{24,8},{1,17},{9,25},{17,1},{25,9},{2,18},{10... | collective-permute-start | bytes 417800 | tf_op jit(solution)/shard_map/ppermute | solution.py:337
  41.3 6.9 %collective-permute-start.2 = (bf16[2,272,128]{2,1,0:T(8,128)(2,1)S(1)}, bf16[2,272,128]{2,1,0:T(8,128)(2,1)S(1)}, u32[]{:S(2)}, u32[]{:S(2)}) collective-permute-start(bf16[2,272,128]{2,1,0:T(8,128)(2,1)S(1)} %copy-done), channel_id=1, source_target_pairs={{0,24},{8,0},{16,8},{24,16},{1,25},{9,1},{17,9},{25,17},{2,26},{10... | collective-permute-start | bytes 417800 | tf_op jit(solution)/shard_map/ppermute | solution.py:337
  61.5 7.8 %collective-permute-start.3 = (bf16[8,144,256]{2,1,0:T(8,128)(2,1)S(1)}, bf16[8,144,256]{2,1,0:T(8,128)(2,1)S(1)}, u32[]{:S(2)}, u32[]{:S(2)}) collective-permute-start(bf16[8,144,256]{2,1,0:T(8,128)(2,1)S(1)} %all-to-all-done.1.own_ref), channel_id=1, source_target_pairs={{0,4},{4,0},{1,5},{5,1},{2,6},{6,2},{3,7},{7,3},{8,12},{12,8},{9,1... | collective-permute-start | bytes 1769480 | tf_op jit(solution)/shard_map/ppermute | solution.py:340
  63.6 25.4 %collective-permute-start.4 = (bf16[8,144,256]{2,1,0:T(8,128)(2,1)S(1)}, bf16[8,144,256]{2,1,0:T(8,128)(2,1)S(1)}, u32[]{:S(2)}, u32[]{:S(2)}) collective-permute-start(bf16[8,144,256]{2,1,0:T(8,128)(2,1)S(1)} %all-to-all-done.1.own_ref), channel_id=1, source_target_pairs={{0,32},{32,0},{1,33},{33,1},{2,34},{34,2},{3,35},{35,3},{4,36},{36... | collective-permute-start | bytes 1769480 | tf_op jit(solution)/shard_map/ppermute | solution.py:339
  89.0 43.0 %collective-permute-start.5 = (bf16[8,144,256]{2,1,0:T(8,128)(2,1)S(1)}, bf16[8,144,256]{2,1,0:T(8,128)(2,1)S(1)}, u32[]{:S(2)}, u32[]{:S(2)}) collective-permute-start(bf16[8,144,256]{2,1,0:T(8,128)(2,1)S(1)} %collective-permute-done.4.own_ref), channel_id=1, source_target_pairs={{0,4},{4,0},{1,5},{5,1},{2,6},{6,2},{3,7},{7,3},{8,12},{12,8},{9,1... | collective-permute-start | bytes 1769480 | tf_op jit(solution)/shard_map/ppermute | solution.py:348
  143.2 15.2 %all-to-all-start.3 = ((bf16[4,72,512]{2,1,0:T(8,128)(2,1)}), bf16[4,72,512]{2,1,0:T(8,128)(2,1)S(1)}, u32[]{:S(2)}, u32[]{:S(2)}) async-start(bf16[4,72,512]{2,1,0:T(8,128)(2,1)} %attend.5), calls=%async_computation.3 | async-start | bytes 589824 | tf_op jit(solution)/shard_map/all_to_all | solution.py:350
  158.4 11.6 %copy-start.1 = (bf16[4,72,512]{2,1,0:T(8,128)(2,1)}, bf16[4,72,512]{2,1,0:T(8,128)(2,1)S(1)}, u32[]{:S(2)}) copy-start(bf16[4,72,512]{2,1,0:T(8,128)(2,1)S(1)} %all-to-all-done.3.late_ref) | copy-start | bytes 884740
where the time goes:
time: 226 us; the launch traced here: 229 us
  blocking collectives  86 us (38%)
  starting transfers between devices  74.2 us (33%)
  Pallas kernels  47.9 us (21%)
  waiting for transfers between devices  18.4 us (8%)
    all_to_all x1, blocking collectives, per_device(): lax.all_to_all(finish(early_shared, late_shared, w_out), 'y', 0, 0, tiled...  54.9 us
    pallas_call x3, Pallas kernels, attend(): pl.pallas_call(functools.partial(attend_kernel, parts), in_specs=[SMEM] +...  41.6 us
    ppermute x1, starting transfers between devices, per_device(): other_swapped = lax.ppermute(other_own, 'c', SWAP)  41.3 us
    all_to_all x1, blocking collectives, sent_to_all(): return lax.all_to_all(copies, axis, split_axis=0, concat_axis=0, tiled=True)  19.5 us
    all_to_all x1, waiting for transfers between devices, per_device(): same_own = lax.all_to_all(copies, 'zh', 0, 0, tiled=True)  13.3 us
    all_to_all x1, blocking collectives, per_device(): early_shared = lax.all_to_all(early, 'x', 0, 0, tiled=True)  11.6 us
    ppermute x3, starting transfers between devices, per_device(): lax.ppermute(queries, 'x', [(i, (i + j) % 4) for i in range(4)])  11.4 us
    all_to_all x1, starting transfers between devices, per_device(): same_own = lax.all_to_all(copies, 'zh', 0, 0, tiled=True)  9.42 us
  transfers between devices with their start and end apart: 8, of which 4 were waited for; matrix products, arithmetic and copies ran while one was open for 0% of the time, Pallas kernels for 13%

commit v1 on v0

--- a/solution.py
+++ b/solution.py
@@ -303,24 +303,43 @@
     return mixed / total
 
 
-def finish_kernel(early_ref, late_ref, w_ref, o_ref):
+def regroup_kernel(early_ref, late_ref, o_ref):
     for part, ref in enumerate((early_ref, late_ref)):
         mixed = merged(ref)
         half = jnp.concatenate([mixed[:, h * HALF : (h + 1) * HALF] for h in range(GROUP)], axis=0)
-        out = jnp.dot(half.T.astype(BF), w_ref[...], preferred_element_type=F32).astype(BF)
+        rows = half.T.astype(BF)
         for y in range(4):
-            o_ref[y, part * 32 : part * 32 + 32, :] = out[y * 32 : y * 32 + 32]
-
-
-def finish(early, late, w_out):
+            o_ref[y, part * 32 : part * 32 + 32, :] = rows[y * 32 : y * 32 + 32]
+
+
+def regroup(early, late):
+    return pl.pallas_call(
+        regroup_kernel,
+        in_specs=[VMEM] * 2,
+        out_specs=VMEM,
+        out_shape=jax.ShapeDtypeStruct((4, 64, GROUP * HD), BF),
+        cost_estimate=pl.CostEstimate(flops=10_000_000, bytes_accessed=1 << 20, transcendentals=0),
+        name="regroup",
+    )(early, late)
+
+
+def finish_kernel(sc_ref, x_ref, w0_ref, w1_ref, w2_ref, w3_ref, o_ref):
+    total = None
+    for j, ref in enumerate((w0_ref, w1_ref, w2_ref, w3_ref)):
+        share = jnp.dot(x_ref[sc_ref[8 + j]], ref[...], preferred_element_type=F32)
+        total = share if total is None else total + share
+    o_ref[...] = total.astype(BF)
+
+
+def finish(scalars, x, weights):
     return pl.pallas_call(
         finish_kernel,
-        in_specs=[VMEM] * 3,
+        in_specs=[SMEM] + [VMEM] * 5,
         out_specs=VMEM,
-        out_shape=jax.ShapeDtypeStruct((4, 64, w_out.shape[1]), BF),
-        cost_estimate=pl.CostEstimate(flops=300_000_000, bytes_accessed=3 << 20, transcendentals=0),
+        out_shape=jax.ShapeDtypeStruct((64, weights[0].shape[1]), BF),
+        cost_estimate=pl.CostEstimate(flops=300_000_000, bytes_accessed=5 << 20, transcendentals=0),
         name="finish",
-    )(early, late, w_out)
+    )(scalars, x, *weights)
 
 
 def sent_to_all(x, axis):
@@ -334,14 +353,21 @@
     rows = sent_to_all(tokens, "y")
     queries, copies = project(rows, w_query, w_key.T, w_value.T, cum_gate)
     same_own = lax.all_to_all(copies, "zh", 0, 0, tiled=True)
-    two, one, three = (lax.ppermute(queries, "x", [(i, (i + j) % 4) for i in range(4)]) for j in (2, 1, 3))
-    same_own, gathered = lax.optimization_barrier((same_own, [queries, one, two, three]))
+    weights = [w_out]
+    gathered = [queries]
+    source, queries = lax.optimization_barrier((w_out, queries))
+    for j in range(1, 4):
+        shift = [(i, (i + j) % 4) for i in range(4)]
+        weights.append(lax.ppermute(source, "y", shift))
+        gathered.append(lax.ppermute(queries, "x", shift))
+    same_own, gathered = lax.optimization_barrier((same_own, gathered))
     other_own = lax.ppermute(same_own, "zl", SWAP)
     same_swapped = lax.ppermute(same_own, "c", SWAP)
     scalars = []
     for parity in (zl, 1 - zl):
         full = (plane - parity + 1) // 2
-        numbers = [full, 1 - (plane - parity) % 2, x * 512, c * ROWS, *((x - j) % 4 for j in range(4))]
+        numbers = [full, 1 - (plane - parity) % 2, x * 512, c * ROWS]
+        numbers += [(at - j) % 4 for at in (x, lax.axis_index("y")) for j in range(4)]
         scalars.append(jnp.stack(numbers).astype(jnp.int32))
     acc0, top0, acc1, top1 = attend(scalars[0], gathered, same_own, same_swapped, (0, 1), ())
     top0, top1, other_own = lax.optimization_barrier((top0, top1, other_own))
@@ -350,8 +376,8 @@
     late_shared = lax.all_to_all(late, "x", 0, 0, tiled=True)
     (early,) = attend(scalars[1], gathered, other_own, other_swapped, (0,), (acc0, top0))
     early_shared = lax.all_to_all(early, "x", 0, 0, tiled=True)
-    pieces = lax.all_to_all(finish(early_shared, late_shared, w_out), "y", 0, 0, tiled=True)
-    return jnp.sum(pieces.astype(F32), axis=0).astype(BF)
+    pieces = lax.all_to_all(regroup(early_shared, late_shared), "y", 0, 0, tiled=True)
+    return finish(scalars[1], pieces, weights)
 
 
 def solution(mesh):

time: 226 us -> 232 us (1.027); the launches traced: 229 us -> 231 us
  blocking collectives: 86 us -> 31 us
  Pallas kernels: 47.9 us -> 89.8 us
  starting transfers between devices: 74.2 us -> 83.6 us
  waiting for transfers between devices: 18.4 us -> 24.1 us
    all_to_all x2 -> x1, blocking collectives: 66.5 us -> 11.6 us  [per_device(): late_shared = lax.all_to_all(late, 'x', 0, 0, tiled=True)]
    all_to_all x1 -> x2, starting transfers between devices: 4.46 us -> 46.5 us  [the longest x1 42.2 us: per_device(): lax.all_to_all(regroup(early_shared, late_shared), 'y', 0, 0, tiled=True)]
    pallas_call x3, Pallas kernels: 41.6 us -> 80.8 us  [attend(): pl.pallas_call(functools.partial(attend_kernel, parts), in_specs=[SMEM] +...]
    ppermute x1, starting transfers between devices: 41.3 us -> 2.12 us  [per_device(): other_swapped = lax.ppermute(other_own, 'c', SWAP)]
    ppermute x3 -> x6, starting transfers between devices: 11.4 us -> 17.9 us  [the longest x3 10.2 us: per_device(): gathered.append(lax.ppermute(queries, 'x', shift))]
    all_to_all x1 -> x2, waiting for transfers between devices: 0.01 us -> 5.96 us  [the longest x1 5.96 us: per_device(): lax.all_to_all(regroup(early_shared, late_shared), 'y', 0, 0, tiled=True)]
    pallas_call x1 -> x2, Pallas kernels: 2.95 us -> 5.7 us  [the longest x1 3.76 us: finish(): pl.pallas_call(finish_kernel, in_specs=[SMEM] + [VMEM] * 5, out_specs=VME...]
    ppermute x3 -> x6, waiting for transfers between devices: 3.59 us -> 5.36 us  [the longest x3 5.35 us: per_device(): gathered.append(lax.ppermute(queries, 'x', shift))]
  transfers between devices with their start and end apart: 8 -> 12, of which waited for: 4 -> 4; matrix products, arithmetic and copies ran while one was open for 0% -> 0% of each run, Pallas kernels for 13% -> 36%
where the time goes in v1:
time: 232 us; the launch traced here: 231 us
  Pallas kernels  89.8 us (39%)
  starting transfers between devices  83.6 us (36%)
  blocking collectives  31 us (13%)
  waiting for transfers between devices  24.1 us (10%)
    pallas_call x3, Pallas kernels, attend(): pl.pallas_call(functools.partial(attend_kernel, parts), in_specs=[SMEM] +...  80.8 us
    all_to_all x1, starting transfers between devices, per_device(): lax.all_to_all(regroup(early_shared, late_shared), 'y', 0, 0, tiled=True)  42.2 us
    all_to_all x1, blocking collectives, sent_to_all(): return lax.all_to_all(copies, axis, split_axis=0, concat_axis=0, tiled=True)  19.5 us
    all_to_all x1, waiting for transfers between devices, per_device(): same_own = lax.all_to_all(copies, 'zh', 0, 0, tiled=True)  12.8 us
    all_to_all x1, blocking collectives, per_device(): late_shared = lax.all_to_all(late, 'x', 0, 0, tiled=True)  11.6 us
    ppermute x3, starting transfers between devices, per_device(): gathered.append(lax.ppermute(queries, 'x', shift))  10.2 us
    all_to_all x1, starting transfers between devices, per_device(): same_own = lax.all_to_all(copies, 'zh', 0, 0, tiled=True)  9.42 us
    ppermute x3, starting transfers between devices, per_device(): weights.append(lax.ppermute(source, 'y', shift))  7.78 us
  transfers between devices with their start and end apart: 12, of which 4 were waited for; matrix products, arithmetic and copies ran while one was open for 0% of the time, Pallas kernels for 36%

profile of v1, /device:TPU:480, one launch (start us, length us, event | category | flops | bytes accessed | tf_op | source)
XLA Modules:
  0.0 230.8 jit_solution(9120540114264635208)
XLA Ops:
  0.0 1.1 broadcast_in_dim.3
  1.1 19.5 %all_to_all.25.x_ref = bf16[4,64,2048]{2,1,0:T(8,128)(2,1)} all-to-all(bf16[4,64,2048]{2,1,0:T(8,128)(2,1)S(1)} %broadcast_in_dim.3), channel_id=1, replica_groups=mesh['zh'=8,'zl'=2,'x'=4,'c'=2,'y'=4] {'y'}, dimensions={0} | all-to-all | bytes 2097152 | tf_op jit(solution)/shard_map/all_to_all | solution.py:347
  20.5 3.3 %project.1 = (bf16[2,272,128]{2,1,0:T(8,128)(2,1)}, bf16[8,144,256]{2,1,0:T(8,128)(2,1)}) custom-call(bf16[4,64,2048]{2,1,0:T(8,128)(2,1)} %all_to_all.25.x_ref, bf16[2048,256]{1,0:T(8,128)(2,1)} %wq_ref.1, bf16[64,2048]{1,0:T(8,128)(2,1)} %bitcast.16, bf16[64,2048]{1,0:T(8,128)(2,1)} %bitcast.17, f32[4,256]{1,0:T(4,128)} %gate_ref.1), custom_call_target="tpu_custom_call" | custom-call | flops 402653184 | bytes 3145728 | tf_op jit(solution)/shard_map/project/pallas_call | solution.py:67
  23.8 0.0 copy-start.1
  23.8 9.4 %all-to-all-start.1 = ((bf16[8,144,256]{2,1,0:T(8,128)(2,1)}), bf16[8,144,256]{2,1,0:T(8,128)(2,1)S(1)}, u32[]{:S(2)}, u32[]{:S(2)}) async-start(bf16[8,144,256]{2,1,0:T(8,128)(2,1)} %get-tuple-element.21), calls=%async_computation.1 | async-start | bytes 1179648 | tf_op jit(solution)/shard_map/all_to_all | solution.py:355
  33.2 0.0 copy-done.1
  33.2 4.7 %collective-permute-start.2 = (bf16[2,272,128]{2,1,0:T(8,128)(2,1)S(1)}, bf16[2,272,128]{2,1,0:T(8,128)(2,1)S(1)}, u32[]{:S(2)}, u32[]{:S(2)}) collective-permute-start(bf16[2,272,128]{2,1,0:T(8,128)(2,1)S(1)} %copy-done.1), channel_id=1, source_target_pairs={{0,24},{8,0},{16,8},{24,16},{1,25},{9,1},{17,9},{25,17},{2,26},{10... | collective-permute-start | bytes 417800 | tf_op jit(solution)/shard_map/ppermute | solution.py:362
  37.9 2.7 %collective-permute-start.1 = (bf16[2,272,128]{2,1,0:T(8,128)(2,1)S(1)}, bf16[2,272,128]{2,1,0:T(8,128)(2,1)S(1)}, u32[]{:S(2)}, u32[]{:S(2)}) collective-permute-start(bf16[2,272,128]{2,1,0:T(8,128)(2,1)S(1)} %copy-done.1), channel_id=1, source_target_pairs={{0,16},{8,24},{16,0},{24,8},{1,17},{9,25},{17,1},{25,9},{2,18},{10... | collective-permute-start | bytes 417800 | tf_op jit(solution)/shard_map/ppermute | solution.py:362
  40.6 2.8 %collective-permute-start = (bf16[2,272,128]{2,1,0:T(8,128)(2,1)S(1)}, bf16[2,272,128]{2,1,0:T(8,128)(2,1)S(1)}, u32[]{:S(2)}, u32[]{:S(2)}) collective-permute-start(bf16[2,272,128]{2,1,0:T(8,128)(2,1)S(1)} %copy-done.1), channel_id=1, source_target_pairs={{0,8},{8,16},{16,24},{24,0},{1,9},{9,17},{17,25},{25,1},{2,10},{10... | collective-permute-start | bytes 417800 | tf_op jit(solution)/shard_map/ppermute | solution.py:362
  43.4 0.0 collective-permute-done.2.q3_ref
  43.4 3.3 %collective-permute-done.1.q2_ref = bf16[2,272,128]{2,1,0:T(8,128)(2,1)S(1)} collective-permute-done((bf16[2,272,128]{2,1,0:T(8,128)(2,1)S(1)}, bf16[2,272,128]{2,1,0:T(8,128)(2,1)S(1)}, u32[]{:S(2)}, u32[]{:S(2)}) %collective-permute-start.1) | collective-permute-done | bytes 139296 | tf_op jit(solution)/shard_map/ppermute | solution.py:362
  46.8 2.0 collective-permute-done.q1_ref
  48.8 12.8 %all-to-all-done.1.own_ref = bf16[8,144,256]{2,1,0:T(8,128)(2,1)S(1)} async-done(((bf16[8,144,256]{2,1,0:T(8,128)(2,1)}), bf16[8,144,256]{2,1,0:T(8,128)(2,1)S(1)}, u32[]{:S(2)}, u32[]{:S(2)}) %all-to-all-start.1) | async-done | bytes 589856 | tf_op jit(solution)/shard_map/all_to_all | solution.py:355
  61.5 1.9 collective-permute-start.3
  63.6 0.1 stack.73.sc_ref
  63.7 5.7 %collective-permute-start.4 = (bf16[8,144,256]{2,1,0:T(8,128)(2,1)S(1)}, bf16[8,144,256]{2,1,0:T(8,128)(2,1)S(1)}, u32[]{:S(2)}, u32[]{:S(2)}) collective-permute-start(bf16[8,144,256]{2,1,0:T(8,128)(2,1)S(1)} %all-to-all-done.1.own_ref), channel_id=1, source_target_pairs={{0,32},{32,0},{1,33},{33,1},{2,34},{34,2},{3,35},{35,3},{4,36},{36... | collective-permute-start | bytes 1769480 | tf_op jit(solution)/shard_map/ppermute | solution.py:364
  69.4 0.0 collective-permute-done.3.swapped_ref
  69.4 58.9 %attend.3 = (f32[4,72,512]{2,1,0:T(8,128)S(1)}, f32[4,1,512]{2,1,0:T(1,128)S(1)}, f32[4,72,512]{2,1,0:T(8,128)S(1)}, f32[4,1,512]{2,1,0:T(1,128)S(1)}) custom-call(s32[12]{0:T(128)S(1)} %stack.73.sc_ref, bf16[2,272,128]{2,1,0:T(8,128)(2,1)S(1)} %copy-done.1, bf16[2,272,128]{2,1,0:T(8,128)(2,1)S(1)} %collective-permute-done.q1_ref, ...), custom_call_target="tpu_custom_call" | custom-call | flops 10000000000 | bytes 4194304 | tf_op jit(solution)/shard_map/attend/pallas_call | solution.py:271
  128.3 0.0 collective-permute-done.4.own_ref
  128.3 2.1 collective-permute-start.5
  130.5 0.1 stack.70.sc_ref
  130.6 0.0 copy-start
  130.6 3.1 %collective-permute-start.8 = (bf16[256,2048]{1,0:T(8,128)(2,1)}, bf16[256,2048]{1,0:T(8,128)(2,1)}, u32[]{:S(2)}, u32[]{:S(2)}) collective-permute-start(bf16[256,2048]{1,0:T(8,128)(2,1)} %w0_ref.1), channel_id=1, source_target_pairs={{0,3},{1,0},{2,1},{3,2},{4,7},{5,4},{6,5},{7,6},{8,11},{9,8},{10,9... | collective-permute-start | bytes 3145736 | tf_op jit(solution)/shard_map/ppermute | solution.py:361
  133.7 2.1 collective-permute-start.7
  135.8 2.6 %collective-permute-start.6 = (bf16[256,2048]{1,0:T(8,128)(2,1)}, bf16[256,2048]{1,0:T(8,128)(2,1)}, u32[]{:S(2)}, u32[]{:S(2)}) collective-permute-start(bf16[256,2048]{1,0:T(8,128)(2,1)} %w0_ref.1), channel_id=1, source_target_pairs={{0,1},{1,2},{2,3},{3,0},{4,5},{5,6},{6,7},{7,4},{8,9},{9,10},{10,1... | collective-permute-start | bytes 3145736 | tf_op jit(solution)/shard_map/ppermute | solution.py:361
  138.4 0.0 collective-permute-done.5.swapped_ref
  138.4 11.2 %attend.4 = bf16[4,72,512]{2,1,0:T(8,128)(2,1)} custom-call(s32[12]{0:T(128)S(1)} %stack.70.sc_ref, bf16[2,272,128]{2,1,0:T(8,128)(2,1)S(1)} %copy-done.1, bf16[2,272,128]{2,1,0:T(8,128)(2,1)S(1)} %collective-permute-done.q1_ref, bf16[2,272,128]{2,1,0:T(8,128)(2,1)S(1)} %collective-permute-done.1.q2_ref, ...), custom_call_target="tpu_custom_call" | custom-call | flops 5000000000 | bytes 4194304 | tf_op jit(solution)/shard_map/attend/pallas_call | solution.py:271
  149.7 4.3 %all-to-all-start.2 = ((bf16[4,72,512]{2,1,0:T(8,128)(2,1)}), bf16[4,72,512]{2,1,0:T(8,128)(2,1)S(1)}, u32[]{:S(2)}, u32[]{:S(2)}) async-start(bf16[4,72,512]{2,1,0:T(8,128)(2,1)} %attend.4), calls=%async_computation.2 | async-start | bytes 589824 | tf_op jit(solution)/shard_map/all_to_all | solution.py:378
  154.0 0.0 copy-done
  154.0 10.7 %attend.5 = bf16[4,72,512]{2,1,0:T(8,128)(2,1)S(1)} custom-call(s32[12]{0:T(128)S(1)} %stack.70.sc_ref, bf16[2,272,128]{2,1,0:T(8,128)(2,1)S(1)} %copy-done.1, bf16[2,272,128]{2,1,0:T(8,128)(2,1)S(1)} %collective-permute-done.q1_ref, bf16[2,272,128]{2,1,0:T(8,128)(2,1)S(1)} %collective-permute-done.1.q2_ref, ...), custom_call_target="tpu_custom_call" | custom-call | flops 5000000000 | bytes 4194304 | tf_op jit(solution)/shard_map/attend/pallas_call | solution.py:271
  164.7 0.0 all-to-all-done.2.early_ref
  164.7 0.0 copy-start.2
  164.7 11.6 %all_to_all.26.late_ref = bf16[4,72,512]{2,1,0:T(8,128)(2,1)} all-to-all(bf16[4,72,512]{2,1,0:T(8,128)(2,1)S(1)} %attend.5), channel_id=1, replica_groups=mesh['zh'=8,'zl'=2,'x'=4,'c'=2,'y'=4] {'x'}, dimensions={0} | all-to-all | bytes 589824 | tf_op jit(solution)/shard_map/all_to_all | solution.py:376
  176.3 0.0 copy-done.2
  176.3 1.9 regroup.1
  178.2 42.2 %all-to-all-start.4 = ((bf16[4,64,256]{2,1,0:T(8,128)(2,1)}), bf16[4,64,256]{2,1,0:T(8,128)(2,1)S(1)}, u32[]{:S(2)}, u32[]{:S(2)}) async-start(bf16[4,64,256]{2,1,0:T(8,128)(2,1)} %regroup.1), calls=%async_computation.4 | async-start | bytes 262144 | tf_op jit(solution)/shard_map/all_to_all | solution.py:379
  220.4 0.0 collective-permute-done.8.w3_ref
  220.4 0.0 collective-permute-done.7.w2_ref
  220.4 0.0 collective-permute-done.6.w1_ref
  220.5 6.0 %all-to-all-done.4.x_ref = bf16[4,64,256]{2,1,0:T(8,128)(2,1)S(1)} async-done(((bf16[4,64,256]{2,1,0:T(8,128)(2,1)}), bf16[4,64,256]{2,1,0:T(8,128)(2,1)S(1)}, u32[]{:S(2)}, u32[]{:S(2)}) %all-to-all-start.4) | async-done | bytes 131104 | tf_op jit(solution)/shard_map/all_to_all | solution.py:379
  226.4 0.0 copy-start.3
  226.4 0.6 copy-done.3
  227.1 3.8 %finish.1 = bf16[64,2048]{1,0:T(8,128)(2,1)} custom-call(s32[12]{0:T(128)} %copy-done, bf16[4,64,256]{2,1,0:T(8,128)(2,1)} %copy-done.3, bf16[256,2048]{1,0:T(8,128)(2,1)} %w0_ref.1, bf16[256,2048]{1,0:T(8,128)(2,1)} %collective-permute-done.6.w1_ref, bf16[256,2048]{1,0:T(8,128)(2,1)} %collective-permute-done.7.w2_ref, ...), custom_call_target="tpu_custom_call" | custom-call | flops 300000000 | bytes 5242880 | tf_op jit(solution)/shard_map/finish/pallas_call | solution.py:335
Async XLA Ops:
  23.8 9.4 %copy-start.1 = (bf16[2,272,128]{2,1,0:T(8,128)(2,1)S(1)}, bf16[2,272,128]{2,1,0:T(8,128)(2,1)}, u32[]{:S(2)}) copy-start(bf16[2,272,128]{2,1,0:T(8,128)(2,1)} %get-tuple-element.24.q0_ref) | copy-start | bytes 417796
  23.8 37.7 %all-to-all-start.1 = ((bf16[8,144,256]{2,1,0:T(8,128)(2,1)}), bf16[8,144,256]{2,1,0:T(8,128)(2,1)S(1)}, u32[]{:S(2)}, u32[]{:S(2)}) async-start(bf16[8,144,256]{2,1,0:T(8,128)(2,1)} %get-tuple-element.21), calls=%async_computation.1 | async-start | bytes 1179648 | tf_op jit(solution)/shard_map/all_to_all | solution.py:355
  33.2 10.2 %collective-permute-start.2 = (bf16[2,272,128]{2,1,0:T(8,128)(2,1)S(1)}, bf16[2,272,128]{2,1,0:T(8,128)(2,1)S(1)}, u32[]{:S(2)}, u32[]{:S(2)}) collective-permute-start(bf16[2,272,128]{2,1,0:T(8,128)(2,1)S(1)} %copy-done.1), channel_id=1, source_target_pairs={{0,24},{8,0},{16,8},{24,16},{1,25},{9,1},{17,9},{25,17},{2,26},{10... | collective-permute-start | bytes 417800 | tf_op jit(solution)/shard_map/ppermute | solution.py:362
  37.9 8.9 %collective-permute-start.1 = (bf16[2,272,128]{2,1,0:T(8,128)(2,1)S(1)}, bf16[2,272,128]{2,1,0:T(8,128)(2,1)S(1)}, u32[]{:S(2)}, u32[]{:S(2)}) collective-permute-start(bf16[2,272,128]{2,1,0:T(8,128)(2,1)S(1)} %copy-done.1), channel_id=1, source_target_pairs={{0,16},{8,24},{16,0},{24,8},{1,17},{9,25},{17,1},{25,9},{2,18},{10... | collective-permute-start | bytes 417800 | tf_op jit(solution)/shard_map/ppermute | solution.py:362
  40.6 8.2 %collective-permute-start = (bf16[2,272,128]{2,1,0:T(8,128)(2,1)S(1)}, bf16[2,272,128]{2,1,0:T(8,128)(2,1)S(1)}, u32[]{:S(2)}, u32[]{:S(2)}) collective-permute-start(bf16[2,272,128]{2,1,0:T(8,128)(2,1)S(1)} %copy-done.1), channel_id=1, source_target_pairs={{0,8},{8,16},{16,24},{24,0},{1,9},{9,17},{17,25},{25,1},{2,10},{10... | collective-permute-start | bytes 417800 | tf_op jit(solution)/shard_map/ppermute | solution.py:362
  61.5 7.9 %collective-permute-start.3 = (bf16[8,144,256]{2,1,0:T(8,128)(2,1)S(1)}, bf16[8,144,256]{2,1,0:T(8,128)(2,1)S(1)}, u32[]{:S(2)}, u32[]{:S(2)}) collective-permute-start(bf16[8,144,256]{2,1,0:T(8,128)(2,1)S(1)} %all-to-all-done.1.own_ref), channel_id=1, source_target_pairs={{0,4},{4,0},{1,5},{5,1},{2,6},{6,2},{3,7},{7,3},{8,12},{12,8},{9,1... | collective-permute-start | bytes 1769480 | tf_op jit(solution)/shard_map/ppermute | solution.py:365
  63.7 64.6 %collective-permute-start.4 = (bf16[8,144,256]{2,1,0:T(8,128)(2,1)S(1)}, bf16[8,144,256]{2,1,0:T(8,128)(2,1)S(1)}, u32[]{:S(2)}, u32[]{:S(2)}) collective-permute-start(bf16[8,144,256]{2,1,0:T(8,128)(2,1)S(1)} %all-to-all-done.1.own_ref), channel_id=1, source_target_pairs={{0,32},{32,0},{1,33},{33,1},{2,34},{34,2},{3,35},{35,3},{4,36},{36... | collective-permute-start | bytes 1769480 | tf_op jit(solution)/shard_map/ppermute | solution.py:364
  128.3 10.1 %collective-permute-start.5 = (bf16[8,144,256]{2,1,0:T(8,128)(2,1)S(1)}, bf16[8,144,256]{2,1,0:T(8,128)(2,1)S(1)}, u32[]{:S(2)}, u32[]{:S(2)}) collective-permute-start(bf16[8,144,256]{2,1,0:T(8,128)(2,1)S(1)} %collective-permute-done.4.own_ref), channel_id=1, source_target_pairs={{0,4},{4,0},{1,5},{5,1},{2,6},{6,2},{3,7},{7,3},{8,12},{12,8},{9,1... | collective-permute-start | bytes 1769480 | tf_op jit(solution)/shard_map/ppermute | solution.py:374
  130.6 23.4 %copy-start = (s32[12]{0:T(128)}, s32[12]{0:T(128)S(1)}, u32[]{:S(2)}) copy-start(s32[12]{0:T(128)S(1)} %stack.70.sc_ref) | copy-start | bytes 148
  130.6 89.8 %collective-permute-start.8 = (bf16[256,2048]{1,0:T(8,128)(2,1)}, bf16[256,2048]{1,0:T(8,128)(2,1)}, u32[]{:S(2)}, u32[]{:S(2)}) collective-permute-start(bf16[256,2048]{1,0:T(8,128)(2,1)} %w0_ref.1), channel_id=1, source_target_pairs={{0,3},{1,0},{2,1},{3,2},{4,7},{5,4},{6,5},{7,6},{8,11},{9,8},{10,9... | collective-permute-start | bytes 3145736 | tf_op jit(solution)/shard_map/ppermute | solution.py:361
  133.7 86.7 %collective-permute-start.7 = (bf16[256,2048]{1,0:T(8,128)(2,1)}, bf16[256,2048]{1,0:T(8,128)(2,1)}, u32[]{:S(2)}, u32[]{:S(2)}) collective-permute-start(bf16[256,2048]{1,0:T(8,128)(2,1)} %w0_ref.1), channel_id=1, source_target_pairs={{0,2},{1,3},{2,0},{3,1},{4,6},{5,7},{6,4},{7,5},{8,10},{9,11},{10,... | collective-permute-start | bytes 3145736 | tf_op jit(solution)/shard_map/ppermute | solution.py:361
  135.8 84.6 %collective-permute-start.6 = (bf16[256,2048]{1,0:T(8,128)(2,1)}, bf16[256,2048]{1,0:T(8,128)(2,1)}, u32[]{:S(2)}, u32[]{:S(2)}) collective-permute-start(bf16[256,2048]{1,0:T(8,128)(2,1)} %w0_ref.1), channel_id=1, source_target_pairs={{0,1},{1,2},{2,3},{3,0},{4,5},{5,6},{6,7},{7,4},{8,9},{9,10},{10,1... | collective-permute-start | bytes 3145736 | tf_op jit(solution)/shard_map/ppermute | solution.py:361
  149.7 15.0 %all-to-all-start.2 = ((bf16[4,72,512]{2,1,0:T(8,128)(2,1)}), bf16[4,72,512]{2,1,0:T(8,128)(2,1)S(1)}, u32[]{:S(2)}, u32[]{:S(2)}) async-start(bf16[4,72,512]{2,1,0:T(8,128)(2,1)} %attend.4), calls=%async_computation.2 | async-start | bytes 589824 | tf_op jit(solution)/shard_map/all_to_all | solution.py:378
  164.7 11.6 %copy-start.2 = (bf16[4,72,512]{2,1,0:T(8,128)(2,1)}, bf16[4,72,512]{2,1,0:T(8,128)(2,1)S(1)}, u32[]{:S(2)}) copy-start(bf16[4,72,512]{2,1,0:T(8,128)(2,1)S(1)} %all-to-all-done.2.early_ref) | copy-start | bytes 884740
  178.2 48.2 %all-to-all-start.4 = ((bf16[4,64,256]{2,1,0:T(8,128)(2,1)}), bf16[4,64,256]{2,1,0:T(8,128)(2,1)S(1)}, u32[]{:S(2)}, u32[]{:S(2)}) async-start(bf16[4,64,256]{2,1,0:T(8,128)(2,1)} %regroup.1), calls=%async_computation.4 | async-start | bytes 262144 | tf_op jit(solution)/shard_map/all_to_all | solution.py:379
  226.4 0.6 copy-start.3
